TPU v7x, 256 devices: a whole 4x4x8 slice. The times are simulated.
256 devices in a mesh: sp: 64 (over z, x, core), tp: 4 (over y).
Axes of the slice: x: 4, y: 4, z: 8, core: 2. Of those that a mesh axis runs over, the one named last changes fastest.
Arguments:
- cot_out: bfloat16 [16384, 2048], P('sp', 'tp'), may hold values from -16 to 16
- route_ids: int32 [16384, 2], P('sp'), may hold values from 0 to 63, all different within a row; in each aligned block of 256 rows (0 to 255, 256 to 511, ...) at most 12 rows name the same one
- route_weight: float32 [16384, 2], P('sp'), may hold values from 0.1 to 1
- expert_inputs: bfloat16 [64, 768, 2048], P('sp'), may hold values from -48 to 48
- w_gate: bfloat16 [64, 2048, 1024], P('sp', None, 'tp'), may hold values from -0.125 to 0.125
- w_up: bfloat16 [64, 2048, 1024], P('sp', None, 'tp'), may hold values from -0.125 to 0.125
- w_down: bfloat16 [64, 1024, 2048], P('sp', 'tp'), may hold values from -0.1875 to 0.1875
- w_proj: bfloat16 [2048, 2048], P('tp'), may hold values from -0.125 to 0.125
- conv_out: bfloat16 [16384, 2048], P('sp', 'tp'), may hold values from -6 to 6
- channel_norm_gain: float32 [2048], P('tp'), may hold values from 0.1 to 1.9
- taps: float32 [31, 2048], P(None, 'tp'), may hold values from -1 to 1
- value_pre: bfloat16 [16384, 2048], P('sp', 'tp'), may hold values from -6 to 6
- gate_pre: bfloat16 [16384, 2048], P('sp', 'tp'), may hold values from -6 to 6
Outputs:
- grad_gate_w: bfloat16 [64, 2048, 1024], P('sp', None, 'tp')
- grad_up_w: bfloat16 [64, 2048, 1024], P('sp', None, 'tp')
- grad_down_w: bfloat16 [64, 1024, 2048], P('sp', 'tp')
- grad_proj: float32 [2048, 2048], P(('tp', 'sp'))
- grad_value: bfloat16 [16384, 2048], P('sp', 'tp')
- grad_gate: bfloat16 [16384, 2048], P('sp', 'tp')
Inputs may be any that keep to these rules, and one draw needn't show every extreme that they name: `route_ids`: among the tokens of one index of sp no expert is chosen more than 12 times, a bound that some block reaches; a token's experts differ.
All inputs are finite; a program needn't handle non-finite values.
Results may differ from a plain program's by a relative error of at most 0.012.
Values may be sent and summed in bfloat16 or wider, within the bound.
No kernel may reach another device: no remote copies, remote signals or barrier semaphores. Data moves between devices by JAX's collectives and lax.ppermute only.
A program may use at most 128 MiB of HBM per device.

v0:
```python
import jax
import jax.numpy as jnp
from jax import lax
from jax.sharding import Mesh
from jax.sharding import PartitionSpec as P

SP = ("sp_0", "sp_1", "sp_2")
TP_SP = ("tp", "sp_0", "sp_1", "sp_2")
clamp_limit = 7.0
swish_alpha = 1.702
norm_epsilon = 1e-05


def in_blocks(value, dim, devices):
    dims = value.shape
    tiles = value.reshape(*dims[:dim], devices, dims[dim] // devices, *dims[dim + 1 :])
    return jnp.moveaxis(tiles, dim, 0)


def sum_at_owner(value, axis, dim):
    tiles = in_blocks(value, dim, lax.axis_size(axis))
    arrived = lax.all_to_all(tiles, axis, split_axis=0, concat_axis=0, tiled=True)
    return arrived.astype(jnp.float32).sum(axis=0)


def from_everyone(value, axis):
    devices = lax.axis_size(axis)
    return lax.all_to_all(
        jnp.broadcast_to(value[None], (devices, *value.shape)), axis, 0, 0, tiled=True
    )


def in_order(tiles, dim):
    dims = list(tiles.shape[1:])
    dims[dim] *= tiles.shape[0]
    return jnp.moveaxis(tiles, 0, dim).reshape(dims)


def collect(value, axis, dim):
    tiles = from_everyone(value, axis)
    return in_order(tiles, dim)


def sum_by_axis(subtotal, axes):
    for axis in axes:
        subtotal = lax.psum_scatter(subtotal, axis, scatter_dimension=0, tiled=True)
    return subtotal


def of_everyone(value, axis):
    return from_everyone(value, axis).sum(axis=0)


def in_one(arrays, axis):
    flat, at, done = (jnp.concatenate([a.reshape(-1) for a in arrays]), 0, [])
    subtotal = of_everyone(flat, axis)
    for a in arrays:
        done.append(subtotal[at : at + a.size].reshape(a.shape))
        at += a.size
    return tuple(done)


def passed_along(value, axis, steps):
    count = lax.axis_size(axis)
    leading, last = (max(0, -steps), min(count, count - steps))
    return lax.ppermute(value, axis, [(source, source + steps) for source in range(leading, last)])


def per_device(
    cot_out,
    route_ids,
    route_weight,
    expert_inputs,
    w_gate,
    w_up,
    w_down,
    w_proj,
    conv_out,
    channel_norm_gain,
    taps,
    value_pre,
    gate_pre,
):
    group_size = lax.axis_size(SP)
    narrow_size = lax.axis_size("tp")
    tok_rows = cot_out.shape[0]
    chosen = route_ids.shape[1]
    slot_rows = expert_inputs.shape[1]
    capacity = slot_rows // group_size
    model_width = expert_inputs.shape[2]
    local_cols = cot_out.shape[1]
    flat_ids = route_ids.reshape(-1)
    expert_hot = (flat_ids[:, None] == jnp.arange(group_size, dtype=jnp.int32)[None, :]).astype(
        jnp.int32
    )
    earlier = jnp.sum((jnp.cumsum(expert_hot, axis=0) - expert_hot) * expert_hot, axis=1)
    dest_rows = flat_ids * capacity + earlier
    flat_weight = route_weight.reshape(-1)[:, None]
    scaled = (flat_weight * jnp.repeat(cot_out, chosen, axis=0).astype(jnp.float32)).astype(
        jnp.bfloat16
    )
    outgoing = (
        jnp.zeros((group_size * capacity, local_cols), jnp.bfloat16).at[dest_rows].set(scaled)
    )
    moved = lax.all_to_all(
        outgoing.reshape(group_size, capacity, local_cols),
        SP,
        split_axis=0,
        concat_axis=0,
        tiled=True,
    )
    arrived = lax.all_gather(moved, "tp", axis=2, tiled=True)
    rows_cot = arrived.reshape(slot_rows, model_width)
    rows_in = expert_inputs[0]
    gate_weight = w_gate[0]
    up_weight = w_up[0]
    down_weight = w_down[0]
    gate_lin = jnp.dot(rows_in, gate_weight, preferred_element_type=jnp.float32)
    up_lin = jnp.dot(rows_in, up_weight, preferred_element_type=jnp.float32)
    gate_c = jnp.minimum(gate_lin, clamp_limit)
    up_c = jnp.clip(up_lin, -clamp_limit, clamp_limit)
    sigma = jax.nn.sigmoid(swish_alpha * gate_c)
    act = ((up_c + 1.0) * gate_c * sigma).astype(jnp.bfloat16)
    grad_down = jnp.dot(act.T, rows_cot, preferred_element_type=jnp.float32).astype(jnp.bfloat16)
    d_act = jnp.dot(rows_cot, down_weight.T, preferred_element_type=jnp.float32)
    up_open = ((up_lin > -clamp_limit) & (up_lin < clamp_limit)).astype(jnp.float32)
    gate_open = (gate_lin < clamp_limit).astype(jnp.float32)
    d_up = (d_act * gate_c * sigma * up_open).astype(jnp.bfloat16)
    d_gate = (
        d_act * (up_c + 1.0) * (sigma + swish_alpha * gate_c * sigma * (1.0 - sigma)) * gate_open
    ).astype(jnp.bfloat16)
    grad_gate_part = jnp.dot(rows_in.T, d_gate, preferred_element_type=jnp.float32).astype(
        jnp.bfloat16
    )
    grad_up_part = jnp.dot(rows_in.T, d_up, preferred_element_type=jnp.float32).astype(jnp.bfloat16)
    partial_value = jnp.dot(d_gate, gate_weight.T, preferred_element_type=jnp.float32)
    partial_value = partial_value + jnp.dot(d_up, up_weight.T, preferred_element_type=jnp.float32)
    input_grad = sum_at_owner(partial_value.astype(jnp.bfloat16), "tp", 1).astype(jnp.bfloat16)
    coming = lax.all_to_all(
        input_grad.reshape(group_size, capacity, local_cols),
        SP,
        split_axis=0,
        concat_axis=0,
        tiled=True,
    )
    picked = coming.reshape(group_size * capacity, local_cols)[dest_rows].astype(jnp.float32)
    summed = jnp.sum(picked.reshape(tok_rows, chosen, local_cols), axis=1)
    mix_grad = (cot_out.astype(jnp.float32) + summed).astype(jnp.bfloat16)
    mix_full = collect(mix_grad, "tp", 1)
    convolution_filter = conv_out.astype(jnp.float32)
    channel_total = local_cols * narrow_size
    first_sum, square_sum = lax.psum(
        (
            jnp.sum(convolution_filter, axis=1),
            jnp.sum(convolution_filter * convolution_filter, axis=1),
        ),
        "tp",
    )
    channel_mean = (first_sum / channel_total)[:, None]
    var = (square_sum / channel_total)[:, None] - channel_mean * channel_mean
    inverse_deviation = lax.rsqrt(var + norm_epsilon)
    normalized_input = (convolution_filter - channel_mean) * inverse_deviation
    normalized_output = normalized_input * channel_norm_gain[None, :]
    sigma_conv = jax.nn.sigmoid(normalized_output)
    act_conv = (normalized_output * sigma_conv).astype(jnp.bfloat16)
    grad_proj = sum_by_axis(
        lax.dot_general(
            act_conv, mix_full, (((0,), (0,)), ((), ())), preferred_element_type=jnp.float32
        ),
        SP,
    )
    d_act_conv = jnp.dot(mix_full, w_proj.T, preferred_element_type=jnp.float32)
    normalized_gradient = (
        d_act_conv
        * sigma_conv
        * (1.0 + normalized_output * (1.0 - sigma_conv))
        * channel_norm_gain[None, :]
    )
    first_term_gradient, second_term_gradient = in_one(
        (
            jnp.sum(normalized_gradient, axis=1),
            jnp.sum(normalized_gradient * normalized_input, axis=1),
        ),
        "tp",
    )
    convolution_gradient = inverse_deviation * (
        normalized_gradient
        - (first_term_gradient / channel_total)[:, None]
        - normalized_input * (second_term_gradient / channel_total)[:, None]
    )
    reach = taps.shape[0]
    following = passed_along(convolution_gradient[: reach - 1], SP, -1)
    extended = jnp.concatenate([convolution_gradient, following], axis=0)
    d_glu = jnp.zeros_like(convolution_gradient)
    for offset in range(reach):
        begin = reach - 1 - offset
        d_glu = d_glu + taps[offset][None, :] * extended[begin : begin + tok_rows]
    gate_sig = jax.nn.sigmoid(gate_pre.astype(jnp.float32))
    grad_value = (d_glu * gate_sig).astype(jnp.bfloat16)
    grad_gate = (d_glu * value_pre.astype(jnp.float32) * gate_sig * (1.0 - gate_sig)).astype(
        jnp.bfloat16
    )
    return (
        grad_gate_part[None],
        grad_up_part[None],
        grad_down[None],
        grad_proj,
        grad_value,
        grad_gate,
    )


def solution(mesh):
    finer = Mesh(mesh.devices.reshape(8, 4, 2, mesh.shape["tp"]), ("sp_0", "sp_1", "sp_2", "tp"))
    placed = (
        P(SP, "tp"),
        P(SP, None),
        P(SP, None),
        P(SP, None, None),
        P(SP, None, "tp"),
        P(SP, None, "tp"),
        P(SP, "tp", None),
        P("tp", None),
        P(SP, "tp"),
        P("tp"),
        P(None, "tp"),
        P(SP, "tp"),
        P(SP, "tp"),
    )
    return jax.shard_map(
        per_device,
        mesh=finer,
        in_specs=placed,
        out_specs=(
            P(SP, None, "tp"),
            P(SP, None, "tp"),
            P(SP, "tp", None),
            P(TP_SP, None),
            P(SP, "tp"),
            P(SP, "tp"),
        ),
        check_vma=False,
    )
```

profile of v0, /device:TPU:1, one launch (start us, length us, event | category | flops | bytes accessed | tf_op | source)
XLA Modules:
  0.0 352.8 jit_solution(16087362731274032509)
XLA Ops:
  7.2 0.8 broadcast_multiply_fusion
  8.1 0.9 copy.48
  9.6 1.2 reduce-window.6
  11.0 2.2 broadcast_in_dim.15
  13.2 2.9 convert_element_type.80
  16.6 4.1 %scatter_custom_fusion = bf16[768,512]{1,0:T(8,128)(2,1)} fusion(s32[512]{0:T(512)S(1)} %bitcast.147, f32[512,512]{1,0:T(8,128)} %convert_element_type.80, f32[512]{0:T(512)S(1)} %mul.447, bf16[]{:T(256)} %constant.12.clone.1), kind=kCustom, calls=%fused_computation.199 | custom fusion | flops 524288 | bytes 1837058 | tf_op jit(solution)/shard_map/scatter | solution.py:103
  20.6 2.1 reshape.100
  22.7 41.2 %all_to_all.26 = bf16[64,12,512]{2,1,0:T(8,128)(2,1)} all-to-all(bf16[64,12,512]{2,1,0:T(8,128)(2,1)} %reshape.100), channel_id=1, replica_groups=mesh['sp_0'=8,'sp_1'=4,'sp_2'=2,'tp'=4] {'sp_0','sp_1','sp_2'}, dimensions={0} | all-to-all | bytes 1572864 | tf_op jit(solution)/shard_map/all_to_all | solution.py:105
  64.0 3.2 fusion.4
  67.2 1.9 fusion.6
  69.1 42.8 %all-gather.2.cloned.1.call-done = bf16[64,12,2048]{2,1,0:T(8,128)(2,1)} async-done(((bf16[64,12,512]{2,1,0:T(8,128)(2,1)}), bf16[64,12,2048]{2,1,0:T(8,128)(2,1)}) %all-gather.2.cloned.1.call-update) | async-done | bytes 3145744 | tf_op jit(solution)/shard_map/all_gather | solution.py:112
  111.9 6.2 %reshape.101 = bf16[768,2048]{1,0:T(8,128)(2,1)} reshape(bf16[64,12,2048]{2,1,0:T(8,128)(2,1)} %all-gather.2.cloned.1.call-done) | data formatting | bytes 6291456 | tf_op jit(solution)/shard_map/reshape | solution.py:113
  118.0 4.1 %select_convert_fusion = (bf16[768,256]{1,0:T(8,128)(2,1)S(1)}, bf16[768,256]{1,0:T(8,128)(2,1)S(1)}) fusion(f32[768,256]{1,0:T(8,128)} %fusion.4, f32[768,256]{1,0:T(8,128)} %fusion.6, bf16[768,2048]{1,0:T(8,128)(2,1)} %reshape.101, bf16[1,256,2048]{2,1,0:T(8,128)(2,1)} %param.19), kind=kOutput, calls=%fused_computation.62 | convolution fusion | flops 809828352 | bytes 6553600 | tf_op jit(solution)/shard_map/dot_general | solution.py:125
  122.2 1.0 fusion.27
  123.7 1.0 add_convert_fusion
  125.0 39.9 %all_to_all.27 = bf16[4,768,512]{2,1,0:T(8,128)(2,1)} all-to-all(bf16[4,768,512]{2,1,0:T(8,128)(2,1)S(1)} %bitcast.113), channel_id=1, replica_groups=mesh['sp_0'=8,'sp_1'=4,'sp_2'=2,'tp'=4] {'tp'}, dimensions={0} | all-to-all | bytes 6291456 | tf_op jit(solution)/shard_map/all_to_all | solution.py:22
  164.9 3.5 reduce_sum.81
  168.4 2.1 reshape.103
  170.5 12.1 %all-to-all-start.2 = ((bf16[64,12,512]{2,1,0:T(8,128)(2,1)}), bf16[64,12,512]{2,1,0:T(8,128)(2,1)}, u32[]{:S(2)}, u32[]{:S(2)}) async-start(bf16[64,12,512]{2,1,0:T(8,128)(2,1)} %reshape.103), calls=%async_computation.2 | async-start | bytes 2097152 | tf_op jit(solution)/shard_map/all_to_all | solution.py:139
  182.6 28.1 %all-to-all-done.2 = bf16[64,12,512]{2,1,0:T(8,128)(2,1)} async-done(((bf16[64,12,512]{2,1,0:T(8,128)(2,1)}), bf16[64,12,512]{2,1,0:T(8,128)(2,1)}, u32[]{:S(2)}, u32[]{:S(2)}) %all-to-all-start.2) | async-done | bytes 786464 | tf_op jit(solution)/shard_map/all_to_all | solution.py:139
  210.6 2.1 reshape.104
  212.7 3.9 %gather_fusion = bf16[512,512]{1,0:T(8,128)(2,1)} fusion(bf16[768,512]{1,0:T(8,128)(2,1)} %reshape.104, s32[1024]{0:T(1024)S(1)} %pad_clamp_fusion), kind=kCustom, calls=%fused_computation | custom fusion | bytes 1050624 | tf_op jit(solution)/shard_map/gather | solution.py:146
  216.6 2.7 reshape.106
  219.2 3.3 reduce_sum.82
  222.5 1.9 add_convert_fusion.1
  224.4 1.8 copy.53
  226.2 2.0 broadcast_in_dim.19
  228.2 4.2 %all-to-all-start.3 = ((bf16[4,256,512]{1,2,0:T(8,128)(2,1)}), bf16[4,256,512]{1,2,0:T(8,128)(2,1)}, u32[]{:S(2)}, u32[]{:S(2)}) async-start(bf16[4,256,512]{1,2,0:T(8,128)(2,1)} %broadcast_in_dim.19), calls=%async_computation.3 | async-start | bytes 2097152 | tf_op jit(solution)/shard_map/all_to_all | solution.py:28
  232.7 15.6 %all-reduce = (f32[256]{0:T(256)S(1)}, f32[256]{0:T(256)S(1)}) all-reduce(f32[256]{0:T(256)S(1)} %get-tuple-element.39, f32[256]{0:T(256)S(1)} %get-tuple-element.38), channel_id=1, replica_groups=mesh['sp_0'=8,'sp_1'=4,'sp_2'=2,'tp'=4] {'tp'}, use_global_device_ids=true, to_apply=%region_7.8 | all-reduce | flops 512 | bytes 4096 | tf_op jit(solution)/shard_map/psum | solution.py:152
  248.3 4.1 %fusion.142 = f32[512,2048]{1,0:T(8,128)} fusion(bf16[256,2048]{0,1:T(8,128)(2,1)} %bitcast.14, bf16[256,512]{1,0:T(8,128)(2,1)S(1)} %copy-done.2, f32[512]{0:T(512)S(1)} %copy-done.11, f32[256]{0:T(256)S(1)} %get-tuple-element.80, f32[256]{0:T(256)S(1)} %get-tuple-element.79), kind=kOutput, calls=%fused_computation.212 | convolution fusion | flops 538050560 | bytes 5509120 | tf_op jit(solution)/shard_map/dot_general | solution.py:167
  252.4 0.8 copy-done.9
  253.2 0.6 fusion.160
  253.8 0.7 fusion.159
  254.5 4.6 %fusion.14 = bf16[1,256,2048]{2,1,0:T(8,128)(2,1)} fusion(bf16[768,2048]{1,0:T(8,128)(2,1)} %reshape.101, f32[768,256]{1,0:T(8,128)} %fusion.6, f32[768,256]{1,0:T(8,128)} %fusion.4), kind=kOutput, calls=%fused_computation.44 | convolution fusion | flops 807796736 | bytes 5767168 | tf_op jit(solution)/shard_map/dot_general | solution.py:124
  259.1 3.0 fusion.157
  262.7 3.2 all-to-all-start.4
  266.0 38.5 %reduce-scatter.4.cloned.1.call-done = f32[64,2048]{1,0:T(8,128)} async-done(((f32[512,2048]{1,0:T(8,128)}), f32[64,2048]{1,0:T(8,128)}) %reduce-scatter.4.cloned.1.call-update) | async-done | bytes 524304 | tf_op jit(solution)/shard_map/reduce_scatter | solution.py:46
  304.5 3.0 fusion.18
  307.6 1.2 fusion.132
  308.8 0.8 copy-done.1
  309.6 2.9 collective-permute-start
  312.5 3.0 fusion.15
  315.5 2.3 copy.55
  317.8 2.3 copy.56
  320.0 7.5 %reduce-scatter.6.cloned.1.call-done = f32[16,2048]{1,0:T(8,128)} async-done(((f32[64,2048]{1,0:T(8,128)}), f32[16,2048]{1,0:T(8,128)}) %reduce-scatter.6.cloned.1.call-update) | async-done | bytes 131088 | tf_op jit(solution)/shard_map/reduce_scatter | solution.py:46
  327.6 11.4 %multiply_convert_fusion.3 = (bf16[256,512]{1,0:T(8,128)(2,1)}, f32[256,512]{1,0:T(8,128)S(1)}) fusion(bf16[256,512]{1,0:T(8,128)(2,1)} %param.24, bf16[256,512]{1,0:T(8,128)(2,1)S(1)} %copy-done.6, f32[256,512]{1,0:T(8,128)} %copy-done.1, f32[512]{0:T(512)} %bitcast.125, f32[30,512]{1,0:T(8,128)S(1)} %collective-permute-done, f32[512]{0:T(512)} %bitcast.126, ...), kind=kLoop, calls=%fused_computation.202 | loop fusion | flops 13238272 | bytes 1959936 | tf_op jit(solution)/shard_map/convert_element_type | solution.py:200
  339.0 0.9 multiply_convert_fusion.4
  339.8 6.4 %reduce-scatter.8.cloned.1.call-done = f32[8,2048]{1,0:T(8,128)} async-done(((f32[16,2048]{1,0:T(8,128)}), f32[8,2048]{1,0:T(8,128)}) %reduce-scatter.8.cloned.1.call-update) | async-done | bytes 65552 | tf_op jit(solution)/shard_map/reduce_scatter | solution.py:46
  (56 shorter events, 3.1 us)
Async XLA Ops:
  7.2 56.8 %copy-start = (bf16[1,768,2048]{2,1,0:T(8,128)(2,1)S(1)}, bf16[1,768,2048]{2,1,0:T(8,128)(2,1)}, u32[]{:S(2)}) copy-start(bf16[1,768,2048]{2,1,0:T(8,128)(2,1)} %param.16) | copy-start | bytes 9437188
  7.2 9.0 %copy-start.10 = (f32[256,2]{0,1:T(2,128)S(1)}, f32[256,2]{0,1:T(2,128)}, u32[]{:S(2)}) copy-start(f32[256,2]{0,1:T(2,128)} %param.15) | copy-start | bytes 6148
  7.2 104.7 %all-gather.2.cloned.1.call-start = ((), (), s32[]{:S(2)}) async-start(), calls=%async_computation.8 | async-start | bytes 5242880 | tf_op jit(solution)/shard_map/all_gather | solution.py:112
  64.0 3.2 copy-start.4
  118.0 4.2 %copy-start.5 = (bf16[1,2048,256]{2,1,0:T(8,128)(2,1)S(1)}, bf16[1,2048,256]{2,1,0:T(8,128)(2,1)}, u32[]{:S(2)}) copy-start(bf16[1,2048,256]{2,1,0:T(8,128)(2,1)} %param.17) | copy-start | bytes 3145732
  122.2 1.1 copy-start.3
  122.2 1.1 copy-start.8
  122.2 1.5 copy-start.7
  170.5 40.2 %all-to-all-start.2 = ((bf16[64,12,512]{2,1,0:T(8,128)(2,1)}), bf16[64,12,512]{2,1,0:T(8,128)(2,1)}, u32[]{:S(2)}, u32[]{:S(2)}) async-start(bf16[64,12,512]{2,1,0:T(8,128)(2,1)} %reshape.103), calls=%async_computation.2 | async-start | bytes 2097152 | tf_op jit(solution)/shard_map/all_to_all | solution.py:139
  219.2 13.3 %copy-start.2 = (bf16[256,512]{1,0:T(8,128)(2,1)S(1)}, bf16[256,512]{1,0:T(8,128)(2,1)}, u32[]{:S(2)}) copy-start(bf16[256,512]{1,0:T(8,128)(2,1)} %param.21) | copy-start | bytes 786436
  219.2 29.0 %copy-start.11 = (f32[512]{0:T(512)S(1)}, f32[512]{0:T(512)}, u32[]{:S(2)}) copy-start(f32[512]{0:T(512)} %param.22) | copy-start | bytes 6148
  228.2 20.1 %all-to-all-start.3 = ((bf16[4,256,512]{1,2,0:T(8,128)(2,1)}), bf16[4,256,512]{1,2,0:T(8,128)(2,1)}, u32[]{:S(2)}, u32[]{:S(2)}) async-start(bf16[4,256,512]{1,2,0:T(8,128)(2,1)} %broadcast_in_dim.19), calls=%async_computation.3 | async-start | bytes 2097152 | tf_op jit(solution)/shard_map/all_to_all | solution.py:28
  232.4 72.0 %reduce-scatter.4.cloned.1.call-start = ((), (), s32[]{:S(2)}) async-start(), calls=%async_computation.9 | async-start | bytes 4718592 | tf_op jit(solution)/shard_map/reduce_scatter | solution.py:46
  252.4 0.8 copy-start.9
  254.5 4.6 %copy-start.12 = (bf16[512,2048]{1,0:T(8,128)(2,1)S(1)}, bf16[512,2048]{1,0:T(8,128)(2,1)}, u32[]{:S(2)}) copy-start(bf16[512,2048]{1,0:T(8,128)(2,1)} %param.20) | copy-start | bytes 6291460
  262.7 44.8 %all-to-all-start.4 = ((f32[4,1,512]{2,1,0:T(1,128)}), f32[4,1,512]{2,1,0:T(1,128)S(1)}, u32[]{:S(2)}, u32[]{:S(2)}) async-start(f32[4,1,512]{2,1,0:T(1,128)} %broadcast_in_dim.20), calls=%async_computation.7 | async-start | bytes 16384 | tf_op jit(solution)/shard_map/all_to_all | solution.py:28
  266.0 61.6 %reduce-scatter.6.cloned.1.call-start = ((), (), s32[]{:S(2)}) async-start(), calls=%async_computation.10 | async-start | bytes 655360 | tf_op jit(solution)/shard_map/reduce_scatter | solution.py:46
  304.5 41.7 %reduce-scatter.8.cloned.1.call-start = ((), (), s32[]{:S(2)}) async-start(), calls=%async_computation.11 | async-start | bytes 196608 | tf_op jit(solution)/shard_map/reduce_scatter | solution.py:46
  308.8 0.8 copy-start.1
  309.6 17.9 %collective-permute-start = (f32[30,512]{1,0:T(8,128)S(1)}, f32[30,512]{1,0:T(8,128)S(1)}, u32[]{:S(2)}, u32[]{:S(2)}) collective-permute-start(f32[30,512]{1,0:T(8,128)S(1)} %slice.267), channel_id=1, source_target_pairs={{4,0},{8,4},{12,8},{16,12},{20,16},{24,20},{28,24},{32,28},{36,32}... | collective-permute-start | bytes 184328 | tf_op jit(solution)/shard_map/ppermute | solution.py:66
  315.5 12.1 %copy-start.6 = (bf16[256,512]{1,0:T(8,128)(2,1)S(1)}, bf16[256,512]{1,0:T(8,128)(2,1)}, u32[]{:S(2)}) copy-start(bf16[256,512]{1,0:T(8,128)(2,1)} %param.25) | copy-start | bytes 786436
Sparse Core Ops, SparseCore 0:
  64.1 47.6 all-gather.1
  252.5 51.9 reduce-scatter.3
  307.0 20.4 reduce-scatter.5
  330.4 15.7 reduce-scatter.7
where the time goes:
time: 354 us; the launch traced here: 353 us
  waiting for transfers between devices  123 us (35%)
  blocking collectives  96.7 us (27%)
  local copies, waits for them, and re-layouts  38.6 us (11%)
  matrix products  28.9 us (8%)
  other arithmetic  28.6 us (8%)
  starting transfers between devices  22.6 us (6%)
  between operations  14.1 us (4%)
    reduce_scatter x3, waiting for transfers between devices, sum_by_axis(): subtotal = lax.psum_scatter(subtotal, axis, scatter_dimension=0, tiled=True)  52.4 us
    all_gather x1, waiting for transfers between devices, per_device(): arrived = lax.all_gather(moved, 'tp', axis=2, tiled=True)  42.8 us
    all_to_all x1, blocking collectives, per_device(): lax.all_to_all(outgoing.reshape(group_size, capacity, local_cols), SP, sp...  41.2 us
    all_to_all x1, blocking collectives, sum_at_owner(): lax.all_to_all(tiles, axis, split_axis=0, concat_axis=0, tiled=True)  39.9 us
    all_to_all x1, waiting for transfers between devices, per_device(): lax.all_to_all(input_grad.reshape(group_size, capacity, local_cols), SP,...  28.1 us
    psum x1, blocking collectives, per_device(): lax.psum((jnp.sum(convolution_filter, axis=1), jnp.sum(convolution_filter...  15.6 us
    all_to_all x1, starting transfers between devices, per_device(): lax.all_to_all(input_grad.reshape(group_size, capacity, local_cols), SP,...  12.1 us
    convert_element_type x1, other arithmetic, per_device(): (d_glu * value_pre.astype(jnp.float32) * gate_sig * (1.0 - gate_sig)).ast...  11.4 us
  transfers between devices with their start and end apart: 8, of which 5 were waited for; matrix products, arithmetic and copies ran while one was open for 11% of the time, Pallas kernels for 0%

commit v1 on v0

--- a/solution.py
+++ b/solution.py
@@ -109,7 +109,9 @@
         concat_axis=0,
         tiled=True,
     )
-    arrived = lax.all_gather(moved, "tp", axis=2, tiled=True)
+    arrived = jnp.concatenate(
+        lax.all_to_all(jnp.stack([moved] * lax.axis_size("tp")), "tp", 0, 0), axis=2
+    )
     rows_cot = arrived.reshape(slot_rows, model_width)
     rows_in = expert_inputs[0]
     gate_weight = w_gate[0]

time: 354 us -> 344 us (0.972)
  waiting for transfers between devices: 123 us -> 112 us
    all_gather x1 -> x0, waiting for transfers between devices: 42.8 us -> none  [per_device(): arrived = lax.all_gather(moved, 'tp', axis=2, tiled=True)]
    all_to_all x0 -> x1, waiting for transfers between devices: none -> 31.6 us  [per_device(): lax.all_to_all(jnp.stack([moved] * lax.axis_size('tp')), 'tp', 0, 0)]
    all_to_all x0 -> x1, starting transfers between devices: none -> 4.82 us  [per_device(): lax.all_to_all(jnp.stack([moved] * lax.axis_size('tp')), 'tp', 0, 0)]
    unnamed x30 -> x39, local copies, waits for them, and re-layouts: 7.7 us -> 9.4 us
where the time goes in v1:
time: 344 us; the launch traced here: 342 us
  waiting for transfers between devices  112 us (33%)
  blocking collectives  95.8 us (28%)
  local copies, waits for them, and re-layouts  41 us (12%)
  other arithmetic  28.6 us (8%)
  matrix products  26.1 us (8%)
  starting transfers between devices  24.1 us (7%)
  between operations  14.1 us (4%)
    reduce_scatter x3, waiting for transfers between devices, sum_by_axis(): subtotal = lax.psum_scatter(subtotal, axis, scatter_dimension=0, tiled=True)  52.7 us
    all_to_all x1, blocking collectives, per_device(): lax.all_to_all(outgoing.reshape(group_size, capacity, local_cols), SP, sp...  41.1 us
    all_to_all x1, blocking collectives, sum_at_owner(): lax.all_to_all(tiles, axis, split_axis=0, concat_axis=0, tiled=True)  39.1 us
    all_to_all x1, waiting for transfers between devices, per_device(): lax.all_to_all(jnp.stack([moved] * lax.axis_size('tp')), 'tp', 0, 0)  31.6 us
    all_to_all x1, waiting for transfers between devices, per_device(): lax.all_to_all(input_grad.reshape(group_size, capacity, local_cols), SP,...  28.1 us
    psum x1, blocking collectives, per_device(): lax.psum((jnp.sum(convolution_filter, axis=1), jnp.sum(convolution_filter...  15.6 us
    convert_element_type x1, other arithmetic, per_device(): (d_glu * value_pre.astype(jnp.float32) * gate_sig * (1.0 - gate_sig)).ast...  11.4 us
    unnamed x39, local copies, waits for them, and re-layouts  9.4 us
  transfers between devices with their start and end apart: 8, of which 5 were waited for; matrix products, arithmetic and copies ran while one was open for 11% of the time, Pallas kernels for 0%

profile of v1, /device:TPU:1, one launch (start us, length us, event | category | flops | bytes accessed | tf_op | source)
XLA Modules:
  0.0 342.2 jit_solution(16583873522453403738)
XLA Ops:
  7.2 0.8 broadcast_multiply_fusion
  8.0 0.9 copy.62
  9.6 1.2 reduce-window.6
  11.0 2.2 broadcast_in_dim.15
  13.2 2.9 convert_element_type.80
  16.6 4.1 %scatter_custom_fusion = bf16[768,512]{1,0:T(8,128)(2,1)} fusion(s32[512]{0:T(512)S(1)} %bitcast.154, f32[512,512]{1,0:T(8,128)} %convert_element_type.80, f32[512]{0:T(512)S(1)} %mul.447, bf16[]{:T(256)} %constant.12.clone.1), kind=kCustom, calls=%fused_computation.199 | custom fusion | flops 524288 | bytes 1837058 | tf_op jit(solution)/shard_map/scatter | solution.py:103
  20.6 2.1 reshape.102
  22.7 41.1 %all_to_all.31 = bf16[64,12,512]{2,1,0:T(8,128)(2,1)S(1)} all-to-all(bf16[64,12,512]{2,1,0:T(8,128)(2,1)} %reshape.102), channel_id=1, replica_groups=mesh['sp_0'=8,'sp_1'=4,'sp_2'=2,'tp'=4] {'sp_0','sp_1','sp_2'}, dimensions={0} | all-to-all | bytes 1572864 | tf_op jit(solution)/shard_map/all_to_all | solution.py:105
  64.3 2.1 stack.2
  66.4 4.8 %all-to-all-start.1 = ((bf16[4,64,12,512]{3,1,2,0:T(8,128)(2,1)}), bf16[4,64,12,512]{3,1,2,0:T(8,128)(2,1)}, u32[]{:S(2)}, u32[]{:S(2)}) async-start(bf16[4,64,12,512]{3,1,2,0:T(8,128)(2,1)} %stack.2), calls=%async_computation.1 | async-start | bytes 6291456 | tf_op jit(solution)/shard_map/all_to_all | solution.py:113
  71.2 3.2 fusion.4
  74.4 1.9 fusion.6
  76.3 31.6 %all-to-all-done.1 = bf16[4,64,12,512]{3,1,2,0:T(8,128)(2,1)} async-done(((bf16[4,64,12,512]{3,1,2,0:T(8,128)(2,1)}), bf16[4,64,12,512]{3,1,2,0:T(8,128)(2,1)}, u32[]{:S(2)}, u32[]{:S(2)}) %all-to-all-start.1) | async-done | bytes 3145760 | tf_op jit(solution)/shard_map/all_to_all | solution.py:113
  107.9 4.3 %copy.67 = bf16[64,12,4,512]{3,2,1,0:T(4,128)(2,1)S(1)} copy(bf16[64,12,4,512]{3,0,1,2:T(8,128)(2,1)} %bitcast.5) | data formatting | bytes 6291456 | tf_op jit(solution)/shard_map/reshape | solution.py:112
  112.2 1.0 copy.78
  113.9 1.4 select_convert_fusion
  115.6 1.0 fusion.27
  116.9 1.0 add_convert_fusion
  118.1 39.1 %all_to_all.32 = bf16[4,768,512]{2,1,0:T(8,128)(2,1)} all-to-all(bf16[4,768,512]{2,1,0:T(8,128)(2,1)S(1)} %bitcast.118), channel_id=1, replica_groups=mesh['sp_0'=8,'sp_1'=4,'sp_2'=2,'tp'=4] {'tp'}, dimensions={0} | all-to-all | bytes 6291456 | tf_op jit(solution)/shard_map/all_to_all | solution.py:22
  157.2 3.5 %reduce_sum.81 = bf16[768,512]{1,0:T(8,128)(2,1)} reduce(bf16[4,768,512]{2,1,0:T(8,128)(2,1)} %all_to_all.32, bf16[]{:T(256)} %constant.12.clone.1), dimensions={0}, to_apply=%region_8.9 | reduce | flops 1179648 | bytes 3932162 | tf_op jit(solution)/shard_map/reduce_sum | solution.py:23
  160.7 2.1 reshape.105
  162.8 9.1 %all-to-all-start.3 = ((bf16[64,12,512]{2,1,0:T(8,128)(2,1)}), bf16[64,12,512]{2,1,0:T(8,128)(2,1)}, u32[]{:S(2)}, u32[]{:S(2)}) async-start(bf16[64,12,512]{2,1,0:T(8,128)(2,1)} %reshape.105), calls=%async_computation.3 | async-start | bytes 2097152 | tf_op jit(solution)/shard_map/all_to_all | solution.py:141
  171.9 28.1 %all-to-all-done.3 = bf16[64,12,512]{2,1,0:T(8,128)(2,1)} async-done(((bf16[64,12,512]{2,1,0:T(8,128)(2,1)}), bf16[64,12,512]{2,1,0:T(8,128)(2,1)}, u32[]{:S(2)}, u32[]{:S(2)}) %all-to-all-start.3) | async-done | bytes 786464 | tf_op jit(solution)/shard_map/all_to_all | solution.py:141
  200.0 2.1 reshape.106
  202.0 3.9 %gather_fusion = bf16[512,512]{1,0:T(8,128)(2,1)} fusion(bf16[768,512]{1,0:T(8,128)(2,1)} %reshape.106, s32[1024]{0:T(1024)S(1)} %pad_clamp_fusion), kind=kCustom, calls=%fused_computation | custom fusion | bytes 1050624 | tf_op jit(solution)/shard_map/gather | solution.py:148
  205.9 2.7 reshape.108
  208.6 3.3 reduce_sum.82
  211.9 1.9 add_convert_fusion.1
  213.7 1.8 copy.69
  215.5 2.0 broadcast_in_dim.19
  217.5 4.2 %all-to-all-start.4 = ((bf16[4,256,512]{1,2,0:T(8,128)(2,1)}), bf16[4,256,512]{1,2,0:T(8,128)(2,1)}, u32[]{:S(2)}, u32[]{:S(2)}) async-start(bf16[4,256,512]{1,2,0:T(8,128)(2,1)} %broadcast_in_dim.19), calls=%async_computation.4 | async-start | bytes 2097152 | tf_op jit(solution)/shard_map/all_to_all | solution.py:28
  222.0 15.6 %all-reduce = (f32[256]{0:T(256)S(1)}, f32[256]{0:T(256)S(1)}) all-reduce(f32[256]{0:T(256)S(1)} %get-tuple-element.45, f32[256]{0:T(256)S(1)} %get-tuple-element.44), channel_id=1, replica_groups=mesh['sp_0'=8,'sp_1'=4,'sp_2'=2,'tp'=4] {'tp'}, use_global_device_ids=true, to_apply=%region_7.8 | all-reduce | flops 512 | bytes 4096 | tf_op jit(solution)/shard_map/psum | solution.py:154
  237.6 4.1 %fusion.142 = f32[512,2048]{1,0:T(8,128)} fusion(bf16[256,2048]{0,1:T(8,128)(2,1)} %bitcast.15, bf16[256,512]{1,0:T(8,128)(2,1)S(1)} %copy-done.3, f32[512]{0:T(512)S(1)} %copy-done.12, f32[256]{0:T(256)S(1)} %get-tuple-element.86, f32[256]{0:T(256)S(1)} %get-tuple-element.85), kind=kOutput, calls=%fused_computation.212 | convolution fusion | flops 538050560 | bytes 5509120 | tf_op jit(solution)/shard_map/dot_general | solution.py:169
  241.7 0.8 copy-done.10
  243.8 4.6 %fusion.14 = bf16[1,256,2048]{2,1,0:T(8,128)(2,1)} fusion(bf16[768,2048]{1,0:T(8,128)(2,1)} %bitcast.121, f32[768,256]{1,0:T(8,128)} %fusion.6, f32[768,256]{1,0:T(8,128)} %fusion.4), kind=kOutput, calls=%fused_computation.44 | convolution fusion | flops 807796736 | bytes 5767168 | tf_op jit(solution)/shard_map/dot_general | solution.py:126
  248.5 3.0 fusion.157
  252.0 3.2 all-to-all-start.5
  255.4 38.5 %reduce-scatter.4.cloned.1.call-done = f32[64,2048]{1,0:T(8,128)} async-done(((f32[512,2048]{1,0:T(8,128)}), f32[64,2048]{1,0:T(8,128)}) %reduce-scatter.4.cloned.1.call-update) | async-done | bytes 524304 | tf_op jit(solution)/shard_map/reduce_scatter | solution.py:46
  293.9 3.0 fusion.18
  296.9 1.2 fusion.132
  299.0 2.6 collective-permute-start
  301.6 3.0 fusion.15
  304.6 2.3 copy.71
  306.9 2.3 copy.72
  309.2 7.7 %reduce-scatter.6.cloned.1.call-done = f32[16,2048]{1,0:T(8,128)} async-done(((f32[64,2048]{1,0:T(8,128)}), f32[16,2048]{1,0:T(8,128)}) %reduce-scatter.6.cloned.1.call-update) | async-done | bytes 131088 | tf_op jit(solution)/shard_map/reduce_scatter | solution.py:46
  316.9 11.4 %multiply_convert_fusion.3 = (bf16[256,512]{1,0:T(8,128)(2,1)}, f32[256,512]{1,0:T(8,128)S(1)}) fusion(bf16[256,512]{1,0:T(8,128)(2,1)} %param.24, bf16[256,512]{1,0:T(8,128)(2,1)S(1)} %copy-done.7, f32[256,512]{1,0:T(8,128)} %copy-done.2, f32[512]{0:T(512)} %bitcast.132, f32[30,512]{1,0:T(8,128)S(1)} %collective-permute-done, f32[512]{0:T(512)} %bitcast.133, ...), kind=kLoop, calls=%fused_computation.202 | loop fusion | flops 13238272 | bytes 1959936 | tf_op jit(solution)/shard_map/convert_element_type | solution.py:202
  328.3 0.9 multiply_convert_fusion.4
  329.2 6.5 %reduce-scatter.8.cloned.1.call-done = f32[8,2048]{1,0:T(8,128)} async-done(((f32[16,2048]{1,0:T(8,128)}), f32[8,2048]{1,0:T(8,128)}) %reduce-scatter.8.cloned.1.call-update) | async-done | bytes 65552 | tf_op jit(solution)/shard_map/reduce_scatter | solution.py:46
  (66 shorter events, 6.2 us)
Async XLA Ops:
  7.2 64.0 %copy-start = (bf16[1,768,2048]{2,1,0:T(8,128)(2,1)S(1)}, bf16[1,768,2048]{2,1,0:T(8,128)(2,1)}, u32[]{:S(2)}) copy-start(bf16[1,768,2048]{2,1,0:T(8,128)(2,1)} %param.16) | copy-start | bytes 9437188
  7.2 9.0 %copy-start.11 = (f32[256,2]{0,1:T(2,128)S(1)}, f32[256,2]{0,1:T(2,128)}, u32[]{:S(2)}) copy-start(f32[256,2]{0,1:T(2,128)} %param.15) | copy-start | bytes 6148
  66.4 41.5 %all-to-all-start.1 = ((bf16[4,64,12,512]{3,1,2,0:T(8,128)(2,1)}), bf16[4,64,12,512]{3,1,2,0:T(8,128)(2,1)}, u32[]{:S(2)}, u32[]{:S(2)}) async-start(bf16[4,64,12,512]{3,1,2,0:T(8,128)(2,1)} %stack.2), calls=%async_computation.1 | async-start | bytes 6291456 | tf_op jit(solution)/shard_map/all_to_all | solution.py:113
  71.2 3.2 copy-start.5
  112.2 1.2 copy-start.14
  112.2 1.4 copy-start.15
  112.2 1.7 copy-start.16
  113.3 2.0 copy-start.1
  113.9 1.7 copy-start.6
  115.4 1.3 copy-start.4
  115.4 1.3 copy-start.9
  115.6 1.2 copy-start.8
  162.8 37.1 %all-to-all-start.3 = ((bf16[64,12,512]{2,1,0:T(8,128)(2,1)}), bf16[64,12,512]{2,1,0:T(8,128)(2,1)}, u32[]{:S(2)}, u32[]{:S(2)}) async-start(bf16[64,12,512]{2,1,0:T(8,128)(2,1)} %reshape.105), calls=%async_computation.3 | async-start | bytes 2097152 | tf_op jit(solution)/shard_map/all_to_all | solution.py:141
  208.6 13.3 %copy-start.3 = (bf16[256,512]{1,0:T(8,128)(2,1)S(1)}, bf16[256,512]{1,0:T(8,128)(2,1)}, u32[]{:S(2)}) copy-start(bf16[256,512]{1,0:T(8,128)(2,1)} %param.21) | copy-start | bytes 786436
  208.6 29.0 %copy-start.12 = (f32[512]{0:T(512)S(1)}, f32[512]{0:T(512)}, u32[]{:S(2)}) copy-start(f32[512]{0:T(512)} %param.22) | copy-start | bytes 6148
  217.5 20.1 %all-to-all-start.4 = ((bf16[4,256,512]{1,2,0:T(8,128)(2,1)}), bf16[4,256,512]{1,2,0:T(8,128)(2,1)}, u32[]{:S(2)}, u32[]{:S(2)}) async-start(bf16[4,256,512]{1,2,0:T(8,128)(2,1)} %broadcast_in_dim.19), calls=%async_computation.4 | async-start | bytes 2097152 | tf_op jit(solution)/shard_map/all_to_all | solution.py:28
  221.8 72.0 %reduce-scatter.4.cloned.1.call-start = ((), (), s32[]{:S(2)}) async-start(), calls=%async_computation.9 | async-start | bytes 4718592 | tf_op jit(solution)/shard_map/reduce_scatter | solution.py:46
  241.7 0.8 copy-start.10
  243.8 4.6 %copy-start.13 = (bf16[512,2048]{1,0:T(8,128)(2,1)S(1)}, bf16[512,2048]{1,0:T(8,128)(2,1)}, u32[]{:S(2)}) copy-start(bf16[512,2048]{1,0:T(8,128)(2,1)} %param.20) | copy-start | bytes 6291460
  252.0 44.8 %all-to-all-start.5 = ((f32[4,1,512]{2,1,0:T(1,128)}), f32[4,1,512]{2,1,0:T(1,128)S(1)}, u32[]{:S(2)}, u32[]{:S(2)}) async-start(f32[4,1,512]{2,1,0:T(1,128)} %broadcast_in_dim.20), calls=%async_computation.8 | async-start | bytes 16384 | tf_op jit(solution)/shard_map/all_to_all | solution.py:28
  255.3 61.6 %reduce-scatter.6.cloned.1.call-start = ((), (), s32[]{:S(2)}) async-start(), calls=%async_computation.10 | async-start | bytes 655360 | tf_op jit(solution)/shard_map/reduce_scatter | solution.py:46
  293.8 41.9 %reduce-scatter.8.cloned.1.call-start = ((), (), s32[]{:S(2)}) async-start(), calls=%async_computation.11 | async-start | bytes 196608 | tf_op jit(solution)/shard_map/reduce_scatter | solution.py:46
  298.1 0.8 copy-start.2
  299.0 18.0 %collective-permute-start = (f32[30,512]{1,0:T(8,128)S(1)}, f32[30,512]{1,0:T(8,128)S(1)}, u32[]{:S(2)}, u32[]{:S(2)}) collective-permute-start(f32[30,512]{1,0:T(8,128)S(1)} %slice.267), channel_id=1, source_target_pairs={{4,0},{8,4},{12,8},{16,12},{20,16},{24,20},{28,24},{32,28},{36,32}... | collective-permute-start | bytes 184328 | tf_op jit(solution)/shard_map/ppermute | solution.py:66
  304.6 12.3 %copy-start.7 = (bf16[256,512]{1,0:T(8,128)(2,1)S(1)}, bf16[256,512]{1,0:T(8,128)(2,1)}, u32[]{:S(2)}) copy-start(bf16[256,512]{1,0:T(8,128)(2,1)} %param.25) | copy-start | bytes 786436
Sparse Core Ops, SparseCore 0:
  241.8 51.9 reduce-scatter.3
  296.3 20.5 reduce-scatter.5
  319.9 15.6 reduce-scatter.7
